TPU v7x, 32 devices: a whole 2x2x4 slice. The times are simulated.
32 devices in a mesh: sp: 4 (over x, core), tp: 8 (over z, y).
Axes of the slice: x: 2, y: 2, z: 4, core: 2. Of those that a mesh axis runs over, the one named last changes fastest.
Arguments:
- latent: bfloat16 [512, 4096], P('sp', 'tp'), may hold values from -60 to 60
- context: bfloat16 [64, 4096], P('sp', 'tp'), may hold values from -6 to 6
- conditioning: bfloat16 [4096], P('sp'), may hold values from -6 to 6
- context_prompt_vector: bfloat16 [4096], P('sp'), may hold values from -6 to 6
- shift_matrix: bfloat16 [4096, 4096], P('tp', 'sp'), may hold values from -0.09375 to 0.09375
- scale_matrix: bfloat16 [4096, 4096], P('tp', 'sp'), may hold values from -0.09375 to 0.09375
- residual_gate_matrix: bfloat16 [4096, 4096], P('tp', 'sp'), may hold values from -0.09375 to 0.09375
- query_matrix: bfloat16 [2048, 4096], P('tp'), may hold values from -0.09375 to 0.09375
- key_matrix: bfloat16 [2048, 4096], P('tp'), may hold values from -0.09375 to 0.09375
- value_matrix: bfloat16 [4096, 4096], P('tp'), may hold values from -0.09375 to 0.09375
- gate_matrix: bfloat16 [4096, 4096], P('tp'), may hold values from -0.09375 to 0.09375
- decay_down_factor: bfloat16 [2, 4096, 16], replicated, may hold values from -0.09375 to 0.09375
- decay_up_factor: bfloat16 [2, 16, 2048], replicated, may hold values from -1.5 to 1.5
- decay_key_bias: float32 [2, 2048], replicated, may hold values from -0.5 to 7
- spike_log_decay: float32 [2, 512, 16], P(None, 'sp'), may hold values from -2.8 to 0
- output_gain: float32 [4096], P('tp'), may hold values from 0.1 to 1.9
- output_matrix: bfloat16 [4096, 4096], P('tp'), may hold values from -0.375 to 0.375
Outputs:
- mixed: bfloat16 [512, 4096], P('sp', 'tp')
All inputs are finite; a program needn't handle non-finite values.
Results may differ from a plain program's by a relative error of at most 0.013.
Values may be sent and summed in bfloat16 or wider, within the bound.
A program may use at most 64 MiB of HBM per device.

v0:
```python
import jax
import jax.numpy as jnp
from jax import lax
from jax.sharding import PartitionSpec as P

D = 4096
HEADS = 16
DK = 128
DECAY_RANK = 16
BLK = 64
VGROUP = 64
epsilon = 1e-05
gate_norm = 16.0
precise = lax.Precision.HIGHEST


def for_sending(value):

    def short(part):
        return part.astype(jnp.bfloat16) if part.dtype == jnp.float32 else part

    return jax.tree.map(short, value)


def from_partner(value, axis, distance):
    return lax.ppermute(value, axis, [(i, i ^ 1 << distance) for i in range(lax.axis_size(axis))])


def carried_in(value, axis, combine, identity, reverse):
    peers, index = (lax.axis_size(axis), lax.axis_index(axis))
    everything = jax.tree.map(
        lambda part, kind: lax.all_gather(part.astype(kind), axis),
        value,
        (jnp.bfloat16, jnp.bfloat16),
    )
    start = jax.tree.map(
        lambda part, zero: jnp.broadcast_to(jnp.asarray(zero, part.dtype), part.shape),
        value,
        identity,
    )

    def turn(k, before):
        at = peers - 1 - k if reverse else k
        reached = at > index if reverse else at < index
        new = combine(
            before, jax.tree.map(lambda part, own: part[at].astype(own.dtype), everything, value)
        )
        return jax.tree.map(lambda a, b: jnp.where(reached, a, b), new, before)

    return lax.fori_loop(0, peers, turn, start)


def linear(rows, weight):
    return lax.dot_general(
        rows, weight, (((1,), (1,)), ((), ())), preferred_element_type=jnp.float32
    )


def modulated(rows, row_sum, row_squares, shift_vec, scale_vec):
    rows_f = rows.astype(jnp.float32)
    mean_val = row_sum / D
    variance = row_squares / D - mean_val * mean_val
    return (
        (rows_f - mean_val) * lax.rsqrt(variance + epsilon) * (1.0 + scale_vec) + shift_vec
    ).astype(jnp.bfloat16)


def reverse_rows(array):
    return jnp.flip(array, axis=0)


def end_state(key_rows, value_rows, log_decay):
    cumulative = jnp.cumsum(log_decay, axis=0)
    totals = cumulative[-1]
    weighted = key_rows * jnp.exp(totals - cumulative)
    return (jnp.exp(totals), jnp.einsum("nhd,nhe->hde", weighted, value_rows, precision=precise))


def combine(earlier, later):
    return (earlier[0] * later[0], later[0][..., None] * earlier[1] + later[1])


def blockwise(queries, key_rows, value_rows, log_decay, carried, block_len):
    length, head_count, _ = queries.shape
    value_width = value_rows.shape[-1]
    blocks = length // block_len

    def shaped(array):
        return array.reshape(blocks, block_len, head_count, array.shape[-1])

    triangle = jnp.tril(jnp.ones((block_len, block_len), jnp.float32))

    def advance(state_now, inputs):
        block_q, block_k, block_v, block_a = inputs
        cumulative = jnp.cumsum(block_a, axis=0)
        block_end = cumulative[-1]
        query_dec = block_q * jnp.exp(cumulative)
        scores = (
            jnp.einsum("ihd,jhd->hij", query_dec, block_k * jnp.exp(-cumulative), precision=precise)
            * triangle
        )
        result = jnp.einsum("hij,jhe->ihe", scores, block_v, precision=precise)
        result = result + jnp.einsum("ihd,hde->ihe", query_dec, state_now, precision=precise)
        state_next = state_now * jnp.exp(block_end)[:, :, None] + jnp.einsum(
            "jhd,jhe->hde", block_k * jnp.exp(block_end - cumulative), block_v, precision=precise
        )
        return (state_next, result)

    _, outputs = lax.scan(
        advance, carried, (shaped(queries), shaped(key_rows), shaped(value_rows), shaped(log_decay))
    )
    return outputs.reshape(length, head_count, value_width)


def head_channels(pieces, per_head, tp_index):
    for bit_number in range(per_head.bit_length() - 1):
        partner = from_partner(
            (for_sending(pieces[0]), for_sending(pieces[1]), for_sending(pieces[2])),
            "tp",
            bit_number,
        )
        upper = tp_index // (1 << bit_number) % 2 == 1
        pieces = tuple(
            (
                jnp.where(
                    upper,
                    jnp.concatenate([theirs, mine], axis=1),
                    jnp.concatenate([mine, theirs], axis=1),
                )
                for mine, theirs in zip(pieces, partner)
            )
        )
    return pieces


def context_totals(fwd_growth, fwd_state, bwd_growth, bwd_state, identity):

    def absorb(carried, piece):
        return (combine(carried, piece), None)

    total_fwd, _ = lax.scan(absorb, identity, (fwd_growth, fwd_state))
    total_bwd, _ = lax.scan(absorb, identity, (bwd_growth, bwd_state), reverse=True)
    return (total_fwd, total_bwd)


def stored(array):
    return lax.optimization_barrier(array.astype(jnp.bfloat16))


def local(
    latent,
    context,
    conditioning,
    context_prompt_vector,
    shift_matrix,
    scale_matrix,
    residual_gate_matrix,
    query_matrix,
    key_matrix,
    value_matrix,
    gate_matrix,
    decay_down_factor,
    decay_up_factor,
    decay_key_bias,
    spike_log_decay,
    output_gain,
    output_matrix,
):
    tp_count = lax.axis_size("tp")
    tp_index = lax.axis_index("tp")
    per_head = max(tp_count // HEADS, 1)
    heads_per_shard = max(HEADS // tp_count, 1)
    leading_head = tp_index // per_head * heads_per_shard
    tok_rows = latent.shape[0]
    conds = jax.nn.silu(
        jnp.stack([conditioning, context_prompt_vector]).astype(jnp.float32)
    ).astype(jnp.bfloat16)
    shifts, scales, gates = lax.psum(
        (
            linear(conds, shift_matrix),
            linear(conds, scale_matrix),
            linear(conds, residual_gate_matrix),
        ),
        "sp",
    )
    down_both = jnp.concatenate([decay_down_factor[0].T, decay_down_factor[1].T], axis=0)
    lat_weights = (query_matrix, key_matrix, value_matrix, gate_matrix, down_both)
    ctx_weights = (key_matrix, value_matrix, down_both)
    lat_f = latent.astype(jnp.float32)
    ctx_f = context.astype(jnp.float32)
    lat_sum, lat_squares, ctx_sum, ctx_squares = lax.psum(
        (
            jnp.sum(lat_f, axis=1, keepdims=True),
            jnp.sum(lat_f * lat_f, axis=1, keepdims=True),
            jnp.sum(ctx_f, axis=1, keepdims=True),
            jnp.sum(ctx_f * ctx_f, axis=1, keepdims=True),
        ),
        "tp",
    )
    latent_normalized = modulated(latent, lat_sum, lat_squares, shifts[0], scales[0])
    normed_ctx = modulated(context, ctx_sum, ctx_squares, shifts[1], scales[1])
    lat_piece = lax.all_gather(latent_normalized, "tp", axis=1, tiled=True)
    ctx_piece = lax.all_gather(normed_ctx, "tp", axis=1, tiled=True)
    lat_new = tuple((linear(lat_piece, weight) for weight in lat_weights))
    ctx_new = tuple((linear(ctx_piece, weight) for weight in ctx_weights))
    query_part, key_part, value_part, gate_part, low_rank_part = lat_new
    ctx_key_part, ctx_value_part, ctx_low = ctx_new
    query_full, key_full, ctx_key_full = head_channels(
        (stored(query_part), stored(key_part), stored(ctx_key_part)), per_head, tp_index
    )

    def split_heads(rows, width):
        return rows.astype(jnp.float32).reshape(rows.shape[0], heads_per_shard, width)

    value_cols = value_part.shape[1] // heads_per_shard
    queries = split_heads(query_full, DK) * DK ** (-0.5)
    key_rows = split_heads(key_full, DK)
    ctx_keys = split_heads(ctx_key_full, DK)
    values_lat = split_heads(stored(value_part), value_cols)
    values_ctx = split_heads(stored(ctx_value_part), value_cols)
    gate_rows = stored(gate_part).astype(jnp.float32)

    def per_head_decay(low_rows, direction):
        up_part = lax.dynamic_slice_in_dim(
            decay_up_factor[direction], leading_head * DK, heads_per_shard * DK, 1
        ).astype(jnp.float32)
        bias_part = lax.dynamic_slice_in_dim(
            decay_key_bias[direction], leading_head * DK, heads_per_shard * DK, 0
        )
        pre_act = jnp.dot(low_rows, up_part, precision=precise) + bias_part
        return (jax.nn.log_sigmoid(pre_act) / gate_norm).reshape(
            low_rows.shape[0], heads_per_shard, DK
        )

    decay_spikes = lax.dynamic_slice_in_dim(spike_log_decay, leading_head, heads_per_shard, 2)
    latent_forward = per_head_decay(low_rank_part[:, :DECAY_RANK], 0) + decay_spikes[0][:, :, None]
    latent_backward = per_head_decay(low_rank_part[:, DECAY_RANK:], 1) + decay_spikes[1][:, :, None]
    ctx_fwd = per_head_decay(ctx_low[:, :DECAY_RANK], 0)
    ctx_bwd = per_head_decay(ctx_low[:, DECAY_RANK:], 1)
    cf_growth, cf_state = end_state(ctx_keys, values_ctx, ctx_fwd)
    cb_growth, cb_state = end_state(
        reverse_rows(ctx_keys), reverse_rows(values_ctx), reverse_rows(ctx_bwd)
    )
    lf_growth, lf_state = end_state(key_rows, values_lat, latent_forward)
    lb_growth, lb_state = end_state(
        reverse_rows(key_rows), reverse_rows(values_lat), reverse_rows(latent_backward)
    )
    identity = (
        jnp.ones((heads_per_shard, DK), jnp.float32),
        jnp.zeros((heads_per_shard, DK, value_cols), jnp.float32),
    )
    ctx_gathered = (
        lax.all_gather(cf_growth[None].astype(jnp.bfloat16), "sp", axis=0, tiled=True).astype(
            jnp.float32
        ),
        lax.all_gather(cf_state[None].astype(jnp.bfloat16), "sp", axis=0, tiled=True).astype(
            jnp.float32
        ),
        lax.all_gather(cb_growth[None].astype(jnp.bfloat16), "sp", axis=0, tiled=True).astype(
            jnp.float32
        ),
        lax.all_gather(cb_state[None].astype(jnp.bfloat16), "sp", axis=0, tiled=True).astype(
            jnp.float32
        ),
    )
    total_fwd, total_bwd = context_totals(
        ctx_gathered[0], ctx_gathered[1], ctx_gathered[2], ctx_gathered[3], identity
    )
    prefix = carried_in((lf_growth, lf_state), "sp", combine, identity, False)
    suffix = carried_in((lb_growth, lb_state), "sp", combine, identity, True)
    start_fwd = combine(total_fwd, prefix)[1]
    start_bwd = combine(total_bwd, suffix)[1]
    zero_state = jnp.zeros((heads_per_shard, DK, value_cols), jnp.float32)

    def direction_out(query_rows, key_list, value_list, log_decay, start_state):
        local_part = blockwise(query_rows, key_list, value_list, log_decay, zero_state, BLK)
        reach = query_rows * jnp.exp(jnp.cumsum(log_decay, axis=0))
        return local_part + jnp.einsum("nhd,hde->nhe", reach, start_state, precision=precise)

    out_fwd = direction_out(queries, key_rows, values_lat, latent_forward, start_fwd)
    out_bwd = reverse_rows(
        direction_out(
            reverse_rows(queries),
            reverse_rows(key_rows),
            reverse_rows(values_lat),
            reverse_rows(latent_backward),
            start_bwd,
        )
    )
    grouped = (out_fwd + out_bwd).reshape(tok_rows, -1, VGROUP)
    grouped = grouped * lax.rsqrt(jnp.mean(grouped * grouped, axis=-1, keepdims=True) + epsilon)
    heads_out = (grouped.reshape(tok_rows, -1) * output_gain * jax.nn.silu(gate_rows)).astype(
        jnp.bfloat16
    )
    branch = linear(lax.all_gather(heads_out, "tp", axis=1, tiled=True), output_matrix)
    return (latent.astype(jnp.float32) + gates[0] * branch).astype(jnp.bfloat16)


def solution(mesh):
    placed = (
        P("sp", "tp"),
        P("sp", "tp"),
        P("sp"),
        P("sp"),
        P("tp", "sp"),
        P("tp", "sp"),
        P("tp", "sp"),
        P("tp", None),
        P("tp", None),
        P("tp", None),
        P("tp", None),
        P(),
        P(),
        P(),
        P(None, "sp", None),
        P("tp"),
        P("tp", None),
    )
    return jax.shard_map(
        local, mesh=mesh, in_specs=placed, out_specs=P("sp", "tp"), check_vma=False
    )
```

profile of v0, /device:TPU:0, one launch (start us, length us, event | category | flops | bytes accessed | tf_op | source)
XLA Modules:
  0.0 266.8 jit_solution(12194387579442730119)
XLA Ops:
  14.8 13.2 %all-reduce.1 = (f32[2,512]{1,0:T(2,128)S(1)}, f32[2,512]{1,0:T(2,128)S(1)}, f32[2,512]{1,0:T(2,128)}) all-reduce(f32[2,512]{1,0:T(2,128)S(1)} %fusion.121, f32[2,512]{1,0:T(2,128)S(1)} %fusion.123, f32[2,512]{1,0:T(2,128)S(1)} %fusion.125), channel_id=1, replica_groups=mesh['sp'=4,'tp'=8] {'sp'}, use_global_device_ids=true, to_apply=%region_6.7 | all-reduce | flops 3072 | bytes 24576 | tf_op jit(solution)/shard_map/psum | solution.py:178
  28.0 21.7 %all-reduce = (f32[128,1]{0,1:T(1,128)S(1)}, f32[128,1]{0,1:T(1,128)S(1)}, f32[16,1]{0,1:T(1,128)S(1)}, f32[16,1]{0,1:T(1,128)S(1)}) all-reduce(f32[128,1]{0,1:T(1,128)S(1)} %bitcast.291, f32[128,1]{0,1:T(1,128)S(1)} %bitcast.290, f32[16,1]{0,1:T(1,128)S(1)} %bitcast.293, f32[16,1]{0,1:T(1,128)S(1)} %bitcast.292), channel_id=1, replica_groups=mesh['sp'=4,'tp'=8] {'tp'}, use_global_device_ids=true, to_apply=%region_4.5 | all-reduce | flops 288 | bytes 2304 | tf_op jit(solution)/shard_map/psum | solution.py:191
  49.7 1.7 fusion.62
  53.5 31.0 %all_gather.45 = bf16[16,4096]{1,0:T(8,128)(2,1)S(1)} all-gather(bf16[16,512]{1,0:T(8,128)(2,1)S(1)} %fusion.89), channel_id=1, replica_groups=mesh['sp'=4,'tp'=8] {'tp'}, dimensions={1}, use_global_device_ids=true | all-gather | bytes 147456 | tf_op jit(solution)/shard_map/all_gather | solution.py:203
  84.9 3.4 %convolution_convert_fusion.8 = bf16[16,512]{1,0:T(8,128)(2,1)S(1)} fusion(bf16[16,4096]{1,0:T(8,128)(2,1)S(1)} %all_gather.45, bf16[512,4096]{1,0:T(8,128)(2,1)} %param.38), kind=kOutput, calls=%fused_computation.96 | convolution fusion | flops 67117056 | bytes 4341760 | tf_op jit(solution)/shard_map/dot_general | solution.py:54
  89.8 5.1 %all_gather.46 = bf16[4,2,128]{2,1,0:T(2,128)(2,1)S(1)} all-gather(bf16[1,2,128]{2,1,0:T(2,128)(2,1)S(1)} %get-tuple-element.728), channel_id=1, replica_groups=mesh['sp'=4,'tp'=8] {'sp'}, dimensions={0}, use_global_device_ids=true | all-gather | bytes 2560 | tf_op jit(solution)/shard_map/all_gather | solution.py:253
  95.8 7.3 %all-gather.1 = bf16[8,128,256]{2,1,0:T(8,128)(2,1)S(1)} all-gather(bf16[2,128,256]{2,1,0:T(8,128)(2,1)S(1)} %convolution_convert_fusion.5), channel_id=3, replica_groups=mesh['sp'=4,'tp'=8] {'sp'}, dimensions={0}, use_global_device_ids=true | all-gather | bytes 655360 | tf_op jit(solution)/shard_map/all_gather | solution.py:256
  106.9 5.0 %all_gather.51 = bf16[4,2,128]{2,1,0:T(2,128)(2,1)S(1)} all-gather(bf16[1,2,128]{2,1,0:T(2,128)(2,1)S(1)} %get-tuple-element.734), channel_id=1, replica_groups=mesh['sp'=4,'tp'=8] {'sp'}, dimensions={0}, use_global_device_ids=true | all-gather | bytes 2560 | tf_op jit(solution)/shard_map/all_gather | solution.py:259
  113.8 7.5 %all-gather.3 = bf16[8,128,256]{2,1,0:T(8,128)(2,1)S(1)} all-gather(bf16[2,128,256]{2,1,0:T(8,128)(2,1)S(1)} %convolution_convert_fusion.4), channel_id=5, replica_groups=mesh['sp'=4,'tp'=8] {'sp'}, dimensions={0}, use_global_device_ids=true | all-gather | bytes 655360 | tf_op jit(solution)/shard_map/all_gather | solution.py:262
  122.4 4.4 %while.91 = (s32[]{:T(128)}, f32[2,128,256]{2,1,0:T(8,128)S(1)}, f32[4,2,128]{2,1,0:T(2,128)S(1)}, f32[4,2,128,256]{3,2,1,0:T(8,128)}, s32[]{:T(128)}, /*index=5*/s32[]{:T(128)}, s32[]{:T(128)}) while((s32[]{:T(128)}, f32[2,128,256]{2,1,0:T(8,128)S(1)}, f32[4,2,128]{2,1,0:T(2,128)S(1)}, f32[4,2,128,256]{3,2,1,0:T(8,128)}, ...), condition=%wide.region_28.29_spmd.clone, body=%wide.region_27.28_spmd.clone.sunk | while | flops 196612 | bytes 789619 | solution.py:142
  127.5 1.8 fusion.70
  129.3 1.7 fusion.74
  133.5 2.1 convolution_convert_fusion.7
  137.0 3.7 %convolution_convert_fusion.2 = bf16[128,512]{1,0:T(8,128)(2,1)S(1)} fusion(bf16[128,4096]{1,0:T(8,128)(2,1)S(1)} %copy-done.1, bf16[512,4096]{1,0:T(8,128)(2,1)} %param.38), kind=kOutput, calls=%fused_computation.85 | convolution fusion | flops 536936448 | bytes 5373952 | tf_op jit(solution)/shard_map/dot_general | solution.py:54
  142.3 3.1 %convolution_convert_fusion.6 = bf16[128,256]{1,0:T(8,128)(2,1)} fusion(bf16[128,4096]{1,0:T(8,128)(2,1)S(1)} %copy-done.1, bf16[256,4096]{1,0:T(8,128)(2,1)} %param.36), kind=kOutput, calls=%fused_computation.94 | convolution fusion | flops 268468224 | bytes 3211264 | tf_op jit(solution)/shard_map/dot_general | solution.py:54
  148.4 4.4 %convolution_convert_fusion = bf16[128,512]{1,0:T(8,128)(2,1)} fusion(bf16[128,4096]{1,0:T(8,128)(2,1)S(1)} %copy-done.1, bf16[512,4096]{1,0:T(8,128)(2,1)} %param.39), kind=kOutput, calls=%fused_computation.83 | convolution fusion | flops 536936448 | bytes 5373952 | tf_op jit(solution)/shard_map/dot_general | solution.py:54
  158.9 2.3 exponential_multiply_fusion.2
  161.9 5.9 %while.89 = (s32[]{:T(128)}, f32[2,128,256]{2,1,0:T(8,128)S(1)}, f32[2,64,2,256]{3,1,0,2:T(8,128)}, f32[2,64,2,128]{3,2,1,0:T(2,128)S(1)}, f32[2,64,2,128]{3,2,1...) while((s32[]{:T(128)}, f32[2,128,256]{2,1,0:T(8,128)S(1)}, ...), condition=%wide.region_22.23_spmd.clone, body=%wide.region_20.22_spmd.clone.sunk | while | flops 139837440 | bytes 2366588 | solution.py:109
  167.8 1.9 copy.96
  169.7 5.1 %all_gather.48 = bf16[4,2,128]{2,1,0:T(2,128)(2,1)S(1)} all-gather(bf16[1,2,128]{2,1,0:T(2,128)(2,1)} %get-tuple-element.724), channel_id=1, replica_groups=mesh['sp'=4,'tp'=8] {'sp'}, dimensions={0}, use_global_device_ids=true | all-gather | bytes 2560 | tf_op jit(solution)/shard_map/all_gather | solution.py:32
  176.1 7.9 %all-gather.2 = bf16[8,128,256]{2,1,0:T(8,128)(2,1)} all-gather(bf16[2,128,256]{2,1,0:T(8,128)(2,1)S(1)} %convolution_convert_fusion.1), channel_id=4, replica_groups=mesh['sp'=4,'tp'=8] {'sp'}, dimensions={0}, use_global_device_ids=true | all-gather | bytes 655360 | tf_op jit(solution)/shard_map/all_gather | solution.py:32
  184.0 4.4 %while.90 = (s32[]{:T(128)}, f32[2,128]{1,0:T(2,128)S(1)}, f32[2,128,256]{2,1,0:T(8,128)S(1)}, s32[]{:T(128)}, bf16[4,2,128]{2,1,0:T(2,128)(2,1)S(1)}, /*index=5...) while((s32[]{:T(128)}, f32[2,128]{1,0:T(2,128)S(1)}, ...), condition=%wide.region_25.26_spmd.clone, body=%wide.region_24.25_spmd.clone.sunk | while | flops 328968 | bytes 660669 | solution.py:50
  188.4 2.4 fusion.46
  190.8 3.1 %rev.38 = f32[128,2,256]{0,2,1:T(8,128)} reverse(f32[128,2,256]{0,2,1:T(8,128)} %fusion.46), dimensions={0} | reverse | bytes 524288 | tf_op jit(solution)/shard_map/jit(_flip)/rev | solution.py:69
  195.8 4.3 %while.86 = (s32[]{:T(128)}, f32[2,128,256]{2,1,0:T(8,128)S(1)}, f32[2,64,2,256]{3,1,0,2:T(8,128)}, f32[2,64,2,128]{3,2,1,0:T(2,128)S(1)}, f32[2,64,2,128]{3,2,1...) while((s32[]{:T(128)}, f32[2,128,256]{2,1,0:T(8,128)S(1)}, ...), condition=%wide.region_9.10_spmd.clone, body=%wide.region_7.9_spmd.clone.sunk | while | flops 139837440 | bytes 2594944 | solution.py:109
  200.1 1.8 copy.86
  201.9 5.0 %all_gather.42 = bf16[4,2,128]{2,1,0:T(2,128)(2,1)S(1)} all-gather(bf16[1,2,128]{2,1,0:T(2,128)(2,1)S(1)} %get-tuple-element.720), channel_id=1, replica_groups=mesh['sp'=4,'tp'=8] {'sp'}, dimensions={0}, use_global_device_ids=true | all-gather | bytes 2560 | tf_op jit(solution)/shard_map/all_gather | solution.py:32
  207.3 7.6 %all-gather = bf16[8,128,256]{2,1,0:T(8,128)(2,1)S(1)} all-gather(bf16[2,128,256]{2,1,0:T(8,128)(2,1)S(1)} %convolution_convert_fusion.3), channel_id=2, replica_groups=mesh['sp'=4,'tp'=8] {'sp'}, dimensions={0}, use_global_device_ids=true | all-gather | bytes 655360 | tf_op jit(solution)/shard_map/all_gather | solution.py:32
  215.7 1.7 fusion.130
  217.8 1.7 fusion.68
  219.5 35.8 %all-gather.9.cloned.1.call-done = bf16[128,4096]{1,0:T(8,128)(2,1)} async-done(((bf16[128,512]{1,0:T(8,128)(2,1)}), bf16[128,4096]{1,0:T(8,128)(2,1)}) %all-gather.9.cloned.1.call-update) | async-done | bytes 1048592 | tf_op jit(solution)/shard_map/all_gather | solution.py:295
  255.3 4.7 %fusion.50 = bf16[128,512]{1,0:T(8,128)(2,1)} fusion(bf16[128,4096]{1,0:T(8,128)(2,1)} %all-gather.9.cloned.1.call-done, bf16[512,4096]{1,0:T(8,128)(2,1)} %param.45, bf16[128,512]{1,0:T(8,128)(2,1)S(1)} %copy-done.11, f32[512]{0:T(512)S(1)} %bitcast.285), kind=kOutput, calls=%fused_computation.87 | convolution fusion | flops 537133056 | bytes 5507072 | tf_op jit(solution)/shard_map/dot_general | solution.py:54
  (210 shorter events, 60.2 us)
Async XLA Ops:
  6.5 82.4 %copy-start = (bf16[256,4096]{1,0:T(8,128)(2,1)S(1)}, bf16[256,4096]{1,0:T(8,128)(2,1)}, u32[]{:S(2)}) copy-start(bf16[256,4096]{1,0:T(8,128)(2,1)} %param.37) | copy-start | bytes 6291460
  6.5 46.8 %copy-start.17 = (bf16[16,512]{1,0:T(8,128)(2,1)S(1)}, bf16[16,512]{1,0:T(8,128)(2,1)}, u32[]{:S(2)}) copy-start(bf16[16,512]{1,0:T(8,128)(2,1)} %param.30) | copy-start | bytes 49156
  6.5 46.7 %copy-start.16 = (bf16[2,16,2048]{2,1,0:T(8,128)(2,1)S(1)}, bf16[2,16,2048]{2,1,0:T(8,128)(2,1)}, u32[]{:S(2)}) copy-start(bf16[2,16,2048]{2,1,0:T(8,128)(2,1)} %param.41) | copy-start | bytes 393220
  6.5 121.0 %all-gather.7.cloned.1.call-start = ((), (), s32[]{:S(2)}) async-start(), calls=%async_computation | async-start | bytes 1179648 | tf_op jit(solution)/shard_map/all_gather | solution.py:202
  51.4 203.9 %all-gather.9.cloned.1.call-start = ((), (), s32[]{:S(2)}) async-start(), calls=%async_computation.1 | async-start | bytes 1179648 | tf_op jit(solution)/shard_map/all_gather | solution.py:295
  53.3 49.8 %copy-start.15 = (bf16[16,4096]{1,0:T(8,128)(2,1)}, bf16[16,4096]{1,0:T(8,128)(2,1)S(1)}, u32[]{:S(2)}) copy-start(bf16[16,4096]{1,0:T(8,128)(2,1)S(1)} %get-tuple-element.713) | copy-start | bytes 393220
  53.3 49.8 %copy-start.18 = (bf16[1,16,2048]{2,1,0:T(8,128)(2,1)}, bf16[1,16,2048]{2,1,0:T(8,128)(2,1)S(1)}, u32[]{:S(2)}) copy-start(bf16[1,16,2048]{2,1,0:T(8,128)(2,1)S(1)} %get-tuple-element.721) | copy-start | bytes 196612
  53.3 49.8 %copy-start.19 = (bf16[1,16,2048]{2,1,0:T(8,128)(2,1)}, bf16[1,16,2048]{2,1,0:T(8,128)(2,1)S(1)}, u32[]{:S(2)}) copy-start(bf16[1,16,2048]{2,1,0:T(8,128)(2,1)S(1)} %get-tuple-element.722) | copy-start | bytes 196612
  84.4 5.4 %copy-start.22 = (f32[1,256]{1,0:T(1,128)}, f32[1,256]{1,0:T(1,128)S(1)}, u32[]{:S(2)}) copy-start(f32[1,256]{1,0:T(1,128)S(1)} %get-tuple-element.747) | copy-start | bytes 3076
  103.9 0.8 copy-start.3
  126.8 0.7 copy-start.5
  127.5 9.4 %copy-start.1 = (bf16[128,4096]{1,0:T(8,128)(2,1)S(1)}, bf16[128,4096]{1,0:T(8,128)(2,1)}, u32[]{:S(2)}) copy-start(bf16[128,4096]{1,0:T(8,128)(2,1)} %all-gather.7.cloned.1.call-done) | copy-start | bytes 3145732
  152.8 9.1 %copy-start.2 = (f32[2,128,256]{2,1,0:T(8,128)S(1)}, f32[2,128,256]{2,1,0:T(8,128)}, u32[]{:S(2)}) copy-start(f32[2,128,256]{2,1,0:T(8,128)} %custom-call.4) | copy-start | bytes 786436
  161.9 22.1 %copy-start.8 = (f32[2,128,256]{2,1,0:T(8,128)S(1)}, f32[2,128,256]{2,1,0:T(8,128)}, u32[]{:S(2)}) copy-start(f32[2,128,256]{2,1,0:T(8,128)} %custom-call.6) | copy-start | bytes 786436
  167.8 20.6 %copy-start.6 = (f32[2,128,256]{2,1,0:T(8,128)S(1)}, f32[2,128,256]{2,1,0:T(8,128)}, u32[]{:S(2)}) copy-start(f32[2,128,256]{2,1,0:T(8,128)} %copy-done.5) | copy-start | bytes 786436
  167.8 28.0 %copy-start.9 = (f32[2,64,2,256]{3,2,1,0:T(2,128)S(1)}, f32[2,64,2,256]{3,2,1,0:T(2,128)}, u32[]{:S(2)}) copy-start(f32[2,64,2,256]{3,2,1,0:T(2,128)} %reshape_reshape.7) | copy-start | bytes 786436
  176.1 17.8 %copy-start.14 = (f32[128,256]{1,0:T(8,128)S(1)}, f32[128,256]{1,0:T(8,128)}, u32[]{:S(2)}) copy-start(f32[128,256]{1,0:T(8,128)} %broadcast_multiply_fusion) | copy-start | bytes 393220
  176.1 19.7 %copy-start.10 = (f32[2,64,2,128]{3,2,1,0:T(2,128)S(1)}, f32[2,64,2,128]{3,2,1,0:T(2,128)}, u32[]{:S(2)}) copy-start(f32[2,64,2,128]{3,2,1,0:T(2,128)} %reshape_reshape.6) | copy-start | bytes 393220
  195.8 11.2 %copy-start.13 = (f32[128,2,128]{2,1,0:T(2,128)S(1)}, f32[128,2,128]{2,1,0:T(2,128)}, u32[]{:S(2)}) copy-start(f32[128,2,128]{2,1,0:T(2,128)} %get-tuple-element.717) | copy-start | bytes 393220
  195.8 19.2 %copy-start.7 = (f32[2,128,256]{2,1,0:T(8,128)S(1)}, f32[2,128,256]{2,1,0:T(8,128)}, u32[]{:S(2)}) copy-start(f32[2,128,256]{2,1,0:T(8,128)} %custom-call.2) | copy-start | bytes 786436
  200.1 15.6 %copy-start.4 = (f32[2,128,256]{2,1,0:T(8,128)S(1)}, f32[2,128,256]{2,1,0:T(8,128)}, u32[]{:S(2)}) copy-start(f32[2,128,256]{2,1,0:T(8,128)} %copy-done.3) | copy-start | bytes 786436
  200.1 17.7 %copy-start.20 = (f32[512]{0:T(512)S(1)}, f32[512]{0:T(512)}, u32[]{:S(2)}) copy-start(f32[512]{0:T(512)} %param.44) | copy-start | bytes 6148
  207.3 8.4 %copy-start.12 = (f32[128,2,256]{0,2,1:T(8,128)S(1)}, f32[128,2,256]{0,2,1:T(8,128)}, u32[]{:S(2)}) copy-start(f32[128,2,256]{0,2,1:T(8,128)} %rev.38) | copy-start | bytes 786436
  207.3 12.2 %copy-start.21 = (f32[2,512]{1,0:T(2,128)S(1)}, f32[2,512]{1,0:T(2,128)}, u32[]{:S(2)}) copy-start(f32[2,512]{1,0:T(2,128)} %get-tuple-element.705) | copy-start | bytes 12292
  207.3 47.9 %copy-start.11 = (bf16[128,512]{1,0:T(8,128)(2,1)S(1)}, bf16[128,512]{1,0:T(8,128)(2,1)}, u32[]{:S(2)}) copy-start(bf16[128,512]{1,0:T(8,128)(2,1)} %param.29) | copy-start | bytes 393220
Sparse Core Ops, SparseCore 0:
  51.5 35.1 all-gather.6
  219.6 35.6 all-gather.8
where the time goes:
time: 269 us; the launch traced here: 267 us
  blocking collectives  116 us (43%)
  matrix products  46.5 us (17%)
  waiting for transfers between devices  35.8 us (13%)
  other arithmetic  28.5 us (11%)
  local copies, waits for them, and re-layouts  25 us (9%)
  between operations  13.9 us (5%)
    all_gather x1, waiting for transfers between devices, local(): lax.all_gather(heads_out, 'tp', axis=1, tiled=True)  35.8 us
    all_gather x1, blocking collectives, local(): ctx_piece = lax.all_gather(normed_ctx, 'tp', axis=1, tiled=True)  31 us
    dot_general x12, matrix products, linear(): lax.dot_general(rows, weight, (((1,), (1,)), ((), ())), preferred_element...  28.7 us
    all_gather x4, blocking collectives, carried_in(): lax.all_gather(part.astype(kind), axis)  25.6 us
    psum x1, blocking collectives, local(): lax.psum((jnp.sum(lat_f, axis=1, keepdims=True), jnp.sum(lat_f * lat_f, a...  21.7 us
    psum x1, blocking collectives, local(): lax.psum((linear(conds, shift_matrix), linear(conds, scale_matrix), linea...  13.2 us
    all_gather x1, blocking collectives, local(): lax.all_gather(cb_state[None].astype(jnp.bfloat16), 'sp', axis=0, tiled=T...  7.46 us
    all_gather x1, blocking collectives, local(): lax.all_gather(cf_state[None].astype(jnp.bfloat16), 'sp', axis=0, tiled=T...  7.28 us
  transfers between devices with their start and end apart: 2, of which 1 were waited for; matrix products, arithmetic and copies ran while one was open for 7% of the time, Pallas kernels for 0%

commit v1 on v0

--- a/solution.py
+++ b/solution.py
@@ -200,7 +200,9 @@
     latent_normalized = modulated(latent, lat_sum, lat_squares, shifts[0], scales[0])
     normed_ctx = modulated(context, ctx_sum, ctx_squares, shifts[1], scales[1])
     lat_piece = lax.all_gather(latent_normalized, "tp", axis=1, tiled=True)
-    ctx_piece = lax.all_gather(normed_ctx, "tp", axis=1, tiled=True)
+    ctx_piece = jnp.concatenate(
+        lax.all_to_all(jnp.stack([normed_ctx] * lax.axis_size("tp")), "tp", 0, 0), axis=1
+    )
     lat_new = tuple((linear(lat_piece, weight) for weight in lat_weights))
     ctx_new = tuple((linear(ctx_piece, weight) for weight in ctx_weights))
     query_part, key_part, value_part, gate_part, low_rank_part = lat_new

time: 269 us -> 249 us (0.926)
  blocking collectives: 116 us -> 85.4 us
  waiting for transfers between devices: 35.8 us -> 40.3 us
  other arithmetic: 28.5 us -> 32.8 us
  starting transfers between devices: 0.04 us -> 3.44 us
    all_gather x1 -> x0, blocking collectives: 31 us -> none  [local(): ctx_piece = lax.all_gather(normed_ctx, 'tp', axis=1, tiled=True)]
    add x8, other arithmetic: 4.77 us -> 8.56 us  [combine(): return (earlier[0] * later[0], later[0][..., None] * earlier[1] + later[1])]
    all_to_all x0 -> x1, waiting for transfers between devices: none -> 3.45 us  [local(): lax.all_to_all(jnp.stack([normed_ctx] * lax.axis_size('tp')), 'tp', 0, 0)]
    all_to_all x0 -> x1, starting transfers between devices: none -> 3.37 us  [local(): lax.all_to_all(jnp.stack([normed_ctx] * lax.axis_size('tp')), 'tp', 0, 0)]
  transfers between devices with their start and end apart: 2 -> 3, of which waited for: 1 -> 2; matrix products, arithmetic and copies ran while one was open for 7% -> 9% of each run, Pallas kernels for 0% -> 0%
where the time goes in v1:
time: 249 us; the launch traced here: 248 us
  blocking collectives  85.4 us (34%)
  matrix products  47.2 us (19%)
  waiting for transfers between devices  40.3 us (16%)
  other arithmetic  32.8 us (13%)
  local copies, waits for them, and re-layouts  23.8 us (10%)
  between operations  13.9 us (6%)
  starting transfers between devices  3.44 us (1%)
    all_gather x1, waiting for transfers between devices, local(): lax.all_gather(heads_out, 'tp', axis=1, tiled=True)  36.8 us
    dot_general x12, matrix products, linear(): lax.dot_general(rows, weight, (((1,), (1,)), ((), ())), preferred_element...  28.7 us
    all_gather x4, blocking collectives, carried_in(): lax.all_gather(part.astype(kind), axis)  25.6 us
    psum x1, blocking collectives, local(): lax.psum((jnp.sum(lat_f, axis=1, keepdims=True), jnp.sum(lat_f * lat_f, a...  21.7 us
    psum x1, blocking collectives, local(): lax.psum((linear(conds, shift_matrix), linear(conds, scale_matrix), linea...  13.2 us
    add x8, other arithmetic, combine(): return (earlier[0] * later[0], later[0][..., None] * earlier[1] + later[1])  8.56 us
    all_gather x1, blocking collectives, local(): lax.all_gather(cb_state[None].astype(jnp.bfloat16), 'sp', axis=0, tiled=T...  7.45 us
    all_gather x1, blocking collectives, local(): lax.all_gather(cf_state[None].astype(jnp.bfloat16), 'sp', axis=0, tiled=T...  7.27 us
  transfers between devices with their start and end apart: 3, of which 2 were waited for; matrix products, arithmetic and copies ran while one was open for 9% of the time, Pallas kernels for 0%

profile of v1, /device:TPU:0, one launch (start us, length us, event | category | flops | bytes accessed | tf_op | source)
XLA Modules:
  0.0 247.5 jit_solution(16109635681564169563)
XLA Ops:
  14.8 13.2 %all-reduce.1 = (f32[2,512]{1,0:T(2,128)S(1)}, f32[2,512]{1,0:T(2,128)S(1)}, f32[2,512]{1,0:T(2,128)}) all-reduce(f32[2,512]{1,0:T(2,128)S(1)} %fusion.121, f32[2,512]{1,0:T(2,128)S(1)} %fusion.123, f32[2,512]{1,0:T(2,128)S(1)} %fusion.125), channel_id=1, replica_groups=mesh['sp'=4,'tp'=8] {'sp'}, use_global_device_ids=true, to_apply=%region_6.7 | all-reduce | flops 3072 | bytes 24576 | tf_op jit(solution)/shard_map/psum | solution.py:178
  28.0 21.7 %all-reduce = (f32[128,1]{0,1:T(1,128)S(1)}, f32[128,1]{0,1:T(1,128)S(1)}, f32[16,1]{0,1:T(1,128)S(1)}, f32[16,1]{0,1:T(1,128)S(1)}) all-reduce(f32[128,1]{0,1:T(1,128)S(1)} %bitcast.298, f32[128,1]{0,1:T(1,128)S(1)} %bitcast.297, f32[16,1]{0,1:T(1,128)S(1)} %bitcast.300, f32[16,1]{0,1:T(1,128)S(1)} %bitcast.299), channel_id=1, replica_groups=mesh['sp'=4,'tp'=8] {'tp'}, use_global_device_ids=true, to_apply=%region_4.5 | all-reduce | flops 288 | bytes 2304 | tf_op jit(solution)/shard_map/psum | solution.py:191
  49.7 1.7 fusion.62
  52.9 3.4 %all-to-all-start = ((bf16[8,16,512]{2,1,0:T(8,128)(2,1)}), bf16[8,16,512]{2,1,0:T(8,128)(2,1)S(1)}, u32[]{:S(2)}, u32[]{:S(2)}) async-start(bf16[8,16,512]{2,1,0:T(8,128)(2,1)} %stack.11), calls=%async_computation | async-start | bytes 262144 | tf_op jit(solution)/shard_map/all_to_all | solution.py:204
  60.1 3.5 %all-to-all-done = bf16[8,16,512]{2,1,0:T(8,128)(2,1)S(1)} async-done(((bf16[8,16,512]{2,1,0:T(8,128)(2,1)}), bf16[8,16,512]{2,1,0:T(8,128)(2,1)S(1)}, u32[]{:S(2)}, u32[]{:S(2)}) %all-to-all-start) | async-done | bytes 131104 | tf_op jit(solution)/shard_map/all_to_all | solution.py:204
  64.7 3.4 %convolution_convert_fusion.8 = bf16[16,512]{1,0:T(8,128)(2,1)S(1)} fusion(bf16[16,4096]{1,0:T(8,128)(2,1)S(1)} %bitcast.278, bf16[512,4096]{1,0:T(8,128)(2,1)} %param.38), kind=kOutput, calls=%fused_computation.96 | convolution fusion | flops 67117056 | bytes 4341760 | tf_op jit(solution)/shard_map/dot_general | solution.py:54
  69.7 5.1 %all_gather.42 = bf16[4,2,128]{2,1,0:T(2,128)(2,1)S(1)} all-gather(bf16[1,2,128]{2,1,0:T(2,128)(2,1)S(1)} %get-tuple-element.728), channel_id=1, replica_groups=mesh['sp'=4,'tp'=8] {'sp'}, dimensions={0}, use_global_device_ids=true | all-gather | bytes 2560 | tf_op jit(solution)/shard_map/all_gather | solution.py:255
  75.2 7.3 %all-gather.1 = bf16[8,128,256]{2,1,0:T(8,128)(2,1)S(1)} all-gather(bf16[2,128,256]{2,1,0:T(8,128)(2,1)S(1)} %convolution_convert_fusion.5), channel_id=3, replica_groups=mesh['sp'=4,'tp'=8] {'sp'}, dimensions={0}, use_global_device_ids=true | all-gather | bytes 655360 | tf_op jit(solution)/shard_map/all_gather | solution.py:258
  83.5 4.4 %while.88 = (s32[]{:T(128)}, f32[2,128,256]{2,1,0:T(8,128)S(1)}, f32[4,2,128]{2,1,0:T(2,128)S(1)}, f32[4,2,128,256]{3,2,1,0:T(8,128)}, s32[]{:T(128)}, /*index=5*/s32[]{:T(128)}) while((s32[]{:T(128)}, f32[2,128,256]{2,1,0:T(8,128)S(1)}, f32[4,2,128]{2,1,0:T(2,128)S(1)}, f32[4,2,128,256]{3,2,1,0:T(8,128)}, s32[]{:T(128)}, ...), condition=%wide.region_19.20_spmd.clone, body=%wide.region_18.19_spmd.clone.sunk | while | flops 196611 | bytes 789599 | solution.py:141
  88.0 5.1 %all_gather.47 = bf16[4,2,128]{2,1,0:T(2,128)(2,1)S(1)} all-gather(bf16[1,2,128]{2,1,0:T(2,128)(2,1)S(1)} %get-tuple-element.734), channel_id=1, replica_groups=mesh['sp'=4,'tp'=8] {'sp'}, dimensions={0}, use_global_device_ids=true | all-gather | bytes 2560 | tf_op jit(solution)/shard_map/all_gather | solution.py:261
  93.5 7.5 %all-gather.3 = bf16[8,128,256]{2,1,0:T(8,128)(2,1)S(1)} all-gather(bf16[2,128,256]{2,1,0:T(8,128)(2,1)S(1)} %convolution_convert_fusion.4), channel_id=5, replica_groups=mesh['sp'=4,'tp'=8] {'sp'}, dimensions={0}, use_global_device_ids=true | all-gather | bytes 655360 | tf_op jit(solution)/shard_map/all_gather | solution.py:264
  102.1 4.4 %while.91 = (s32[]{:T(128)}, f32[2,128,256]{2,1,0:T(8,128)S(1)}, f32[4,2,128]{2,1,0:T(2,128)S(1)}, f32[4,2,128,256]{3,2,1,0:T(8,128)}, s32[]{:T(128)}, /*index=5*/s32[]{:T(128)}, s32[]{:T(128)}) while((s32[]{:T(128)}, f32[2,128,256]{2,1,0:T(8,128)S(1)}, f32[4,2,128]{2,1,0:T(2,128)S(1)}, f32[4,2,128,256]{3,2,1,0:T(8,128)}, ...), condition=%wide.region_28.29_spmd.clone, body=%wide.region_27.28_spmd.clone.sunk | while | flops 196612 | bytes 789619 | solution.py:142
  107.2 1.8 fusion.70
  109.0 1.7 fusion.74
  113.2 2.1 convolution_convert_fusion.7
  116.7 3.7 %convolution_convert_fusion.2 = bf16[128,512]{1,0:T(8,128)(2,1)S(1)} fusion(bf16[128,4096]{1,0:T(8,128)(2,1)S(1)} %copy-done.1, bf16[512,4096]{1,0:T(8,128)(2,1)} %param.38), kind=kOutput, calls=%fused_computation.85 | convolution fusion | flops 536936448 | bytes 5373952 | tf_op jit(solution)/shard_map/dot_general | solution.py:54
  122.0 3.1 %convolution_convert_fusion.6 = bf16[128,256]{1,0:T(8,128)(2,1)} fusion(bf16[128,4096]{1,0:T(8,128)(2,1)S(1)} %copy-done.1, bf16[256,4096]{1,0:T(8,128)(2,1)} %param.36), kind=kOutput, calls=%fused_computation.94 | convolution fusion | flops 268468224 | bytes 3211264 | tf_op jit(solution)/shard_map/dot_general | solution.py:54
  128.1 4.4 %convolution_convert_fusion = bf16[128,512]{1,0:T(8,128)(2,1)} fusion(bf16[128,4096]{1,0:T(8,128)(2,1)S(1)} %copy-done.1, bf16[512,4096]{1,0:T(8,128)(2,1)} %param.39), kind=kOutput, calls=%fused_computation.83 | convolution fusion | flops 536936448 | bytes 5373952 | tf_op jit(solution)/shard_map/dot_general | solution.py:54
  138.6 2.3 exponential_multiply_fusion.2
  141.6 5.9 %while.89 = (s32[]{:T(128)}, f32[2,128,256]{2,1,0:T(8,128)S(1)}, f32[2,64,2,256]{3,1,0,2:T(8,128)}, f32[2,64,2,128]{3,2,1,0:T(2,128)S(1)}, f32[2,64,2,128]{3,2,1...) while((s32[]{:T(128)}, f32[2,128,256]{2,1,0:T(8,128)S(1)}, ...), condition=%wide.region_22.23_spmd.clone, body=%wide.region_20.22_spmd.clone.sunk | while | flops 139837440 | bytes 2366588 | solution.py:109
  147.5 1.9 copy.97
  149.4 5.1 %all_gather.44 = bf16[4,2,128]{2,1,0:T(2,128)(2,1)S(1)} all-gather(bf16[1,2,128]{2,1,0:T(2,128)(2,1)} %get-tuple-element.724), channel_id=1, replica_groups=mesh['sp'=4,'tp'=8] {'sp'}, dimensions={0}, use_global_device_ids=true | all-gather | bytes 2560 | tf_op jit(solution)/shard_map/all_gather | solution.py:32
  155.8 7.9 %all-gather.2 = bf16[8,128,256]{2,1,0:T(8,128)(2,1)} all-gather(bf16[2,128,256]{2,1,0:T(8,128)(2,1)S(1)} %convolution_convert_fusion.1), channel_id=4, replica_groups=mesh['sp'=4,'tp'=8] {'sp'}, dimensions={0}, use_global_device_ids=true | all-gather | bytes 655360 | tf_op jit(solution)/shard_map/all_gather | solution.py:32
  163.7 4.4 %while.90 = (s32[]{:T(128)}, f32[2,128]{1,0:T(2,128)S(1)}, f32[2,128,256]{2,1,0:T(8,128)S(1)}, s32[]{:T(128)}, bf16[4,2,128]{2,1,0:T(2,128)(2,1)S(1)}, /*index=5...) while((s32[]{:T(128)}, f32[2,128]{1,0:T(2,128)S(1)}, ...), condition=%wide.region_25.26_spmd.clone, body=%wide.region_24.25_spmd.clone.sunk | while | flops 328968 | bytes 660669 | solution.py:50
  168.1 2.4 fusion.46
  170.5 3.1 %rev.38 = f32[128,2,256]{0,2,1:T(8,128)} reverse(f32[128,2,256]{0,2,1:T(8,128)} %fusion.46), dimensions={0} | reverse | bytes 524288 | tf_op jit(solution)/shard_map/jit(_flip)/rev | solution.py:69
  175.5 4.3 %while.86 = (s32[]{:T(128)}, f32[2,128,256]{2,1,0:T(8,128)S(1)}, f32[2,64,2,256]{3,1,0,2:T(8,128)}, f32[2,64,2,128]{3,2,1,0:T(2,128)S(1)}, f32[2,64,2,128]{3,2,1...) while((s32[]{:T(128)}, f32[2,128,256]{2,1,0:T(8,128)S(1)}, ...), condition=%wide.region_9.10_spmd.clone, body=%wide.region_7.9_spmd.clone.sunk | while | flops 139837440 | bytes 2594944 | solution.py:109
  179.8 1.8 copy.87
  181.6 5.0 %all_gather.39 = bf16[4,2,128]{2,1,0:T(2,128)(2,1)S(1)} all-gather(bf16[1,2,128]{2,1,0:T(2,128)(2,1)S(1)} %get-tuple-element.720), channel_id=1, replica_groups=mesh['sp'=4,'tp'=8] {'sp'}, dimensions={0}, use_global_device_ids=true | all-gather | bytes 2560 | tf_op jit(solution)/shard_map/all_gather | solution.py:32
  187.0 7.6 %all-gather = bf16[8,128,256]{2,1,0:T(8,128)(2,1)S(1)} all-gather(bf16[2,128,256]{2,1,0:T(8,128)(2,1)S(1)} %convolution_convert_fusion.3), channel_id=2, replica_groups=mesh['sp'=4,'tp'=8] {'sp'}, dimensions={0}, use_global_device_ids=true | all-gather | bytes 655360 | tf_op jit(solution)/shard_map/all_gather | solution.py:32
  199.2 36.8 %all-gather.9.cloned.1.call-done = bf16[128,4096]{1,0:T(8,128)(2,1)} async-done(((bf16[128,512]{1,0:T(8,128)(2,1)}), bf16[128,4096]{1,0:T(8,128)(2,1)}) %all-gather.9.cloned.1.call-update) | async-done | bytes 1048592 | tf_op jit(solution)/shard_map/all_gather | solution.py:297
  236.0 4.7 %fusion.50 = bf16[128,512]{1,0:T(8,128)(2,1)} fusion(bf16[128,4096]{1,0:T(8,128)(2,1)} %all-gather.9.cloned.1.call-done, bf16[512,4096]{1,0:T(8,128)(2,1)} %param.45, bf16[128,512]{1,0:T(8,128)(2,1)S(1)} %copy-done.11, f32[512]{0:T(512)S(1)} %bitcast.292), kind=kOutput, calls=%fused_computation.87 | convolution fusion | flops 537133056 | bytes 5507072 | tf_op jit(solution)/shard_map/dot_general | solution.py:54
  (209 shorter events, 66.7 us)
Async XLA Ops:
  6.5 61.6 %copy-start = (bf16[256,4096]{1,0:T(8,128)(2,1)S(1)}, bf16[256,4096]{1,0:T(8,128)(2,1)}, u32[]{:S(2)}) copy-start(bf16[256,4096]{1,0:T(8,128)(2,1)} %param.37) | copy-start | bytes 6291460
  6.5 49.8 %copy-start.16 = (bf16[2,4096,16]{1,2,0:T(8,128)(2,1)S(1)}, bf16[2,4096,16]{1,2,0:T(8,128)(2,1)}, u32[]{:S(2)}) copy-start(bf16[2,4096,16]{1,2,0:T(8,128)(2,1)} %param.40) | copy-start | bytes 786436
  6.5 49.8 %copy-start.17 = (bf16[2,16,2048]{2,1,0:T(8,128)(2,1)S(1)}, bf16[2,16,2048]{2,1,0:T(8,128)(2,1)}, u32[]{:S(2)}) copy-start(bf16[2,16,2048]{2,1,0:T(8,128)(2,1)} %param.41) | copy-start | bytes 393220
  6.5 50.5 %copy-start.18 = (f32[2,2048]{1,0:T(2,128)S(1)}, f32[2,2048]{1,0:T(2,128)}, u32[]{:S(2)}) copy-start(f32[2,2048]{1,0:T(2,128)} %param.42) | copy-start | bytes 49156
  6.5 100.7 %all-gather.7.cloned.1.call-start = ((), (), s32[]{:S(2)}) async-start(), calls=%async_computation.1 | async-start | bytes 1179648 | tf_op jit(solution)/shard_map/all_gather | solution.py:202
  52.9 10.7 %all-to-all-start = ((bf16[8,16,512]{2,1,0:T(8,128)(2,1)}), bf16[8,16,512]{2,1,0:T(8,128)(2,1)S(1)}, u32[]{:S(2)}, u32[]{:S(2)}) async-start(bf16[8,16,512]{2,1,0:T(8,128)(2,1)} %stack.11), calls=%async_computation | async-start | bytes 262144 | tf_op jit(solution)/shard_map/all_to_all | solution.py:204
  56.3 179.7 %all-gather.9.cloned.1.call-start = ((), (), s32[]{:S(2)}) async-start(), calls=%async_computation.2 | async-start | bytes 1179648 | tf_op jit(solution)/shard_map/all_gather | solution.py:297
  56.4 18.8 %copy-start.15 = (bf16[16,4096]{1,0:T(8,128)(2,1)}, bf16[16,4096]{1,0:T(8,128)(2,1)S(1)}, u32[]{:S(2)}) copy-start(bf16[16,4096]{1,0:T(8,128)(2,1)S(1)} %get-tuple-element.713) | copy-start | bytes 393220
  88.0 18.5 %copy-start.5 = (f32[2,128,256]{2,1,0:T(8,128)}, f32[2,128,256]{2,1,0:T(8,128)S(1)}, u32[]{:S(2)}) copy-start(f32[2,128,256]{2,1,0:T(8,128)S(1)} %get-tuple-element.462) | copy-start | bytes 786436
  106.5 0.7 copy-start.3
  107.2 9.4 %copy-start.1 = (bf16[128,4096]{1,0:T(8,128)(2,1)S(1)}, bf16[128,4096]{1,0:T(8,128)(2,1)}, u32[]{:S(2)}) copy-start(bf16[128,4096]{1,0:T(8,128)(2,1)} %all-gather.7.cloned.1.call-done) | copy-start | bytes 3145732
  132.5 9.1 %copy-start.2 = (f32[2,128,256]{2,1,0:T(8,128)S(1)}, f32[2,128,256]{2,1,0:T(8,128)}, u32[]{:S(2)}) copy-start(f32[2,128,256]{2,1,0:T(8,128)} %custom-call.4) | copy-start | bytes 786436
  141.6 22.1 %copy-start.8 = (f32[2,128,256]{2,1,0:T(8,128)S(1)}, f32[2,128,256]{2,1,0:T(8,128)}, u32[]{:S(2)}) copy-start(f32[2,128,256]{2,1,0:T(8,128)} %custom-call.6) | copy-start | bytes 786436
  147.5 20.6 %copy-start.4 = (f32[2,128,256]{2,1,0:T(8,128)S(1)}, f32[2,128,256]{2,1,0:T(8,128)}, u32[]{:S(2)}) copy-start(f32[2,128,256]{2,1,0:T(8,128)} %copy-done.3) | copy-start | bytes 786436
  147.5 28.0 %copy-start.9 = (f32[2,64,2,256]{3,2,1,0:T(2,128)S(1)}, f32[2,64,2,256]{3,2,1,0:T(2,128)}, u32[]{:S(2)}) copy-start(f32[2,64,2,256]{3,2,1,0:T(2,128)} %reshape_reshape.7) | copy-start | bytes 786436
  155.8 17.8 %copy-start.14 = (f32[128,256]{1,0:T(8,128)S(1)}, f32[128,256]{1,0:T(8,128)}, u32[]{:S(2)}) copy-start(f32[128,256]{1,0:T(8,128)} %broadcast_multiply_fusion) | copy-start | bytes 393220
  155.8 19.7 %copy-start.10 = (f32[2,64,2,128]{3,2,1,0:T(2,128)S(1)}, f32[2,64,2,128]{3,2,1,0:T(2,128)}, u32[]{:S(2)}) copy-start(f32[2,64,2,128]{3,2,1,0:T(2,128)} %reshape_reshape.6) | copy-start | bytes 393220
  175.5 11.2 %copy-start.13 = (f32[128,2,128]{2,1,0:T(2,128)S(1)}, f32[128,2,128]{2,1,0:T(2,128)}, u32[]{:S(2)}) copy-start(f32[128,2,128]{2,1,0:T(2,128)} %get-tuple-element.717) | copy-start | bytes 393220
  175.5 19.2 %copy-start.7 = (f32[2,128,256]{2,1,0:T(8,128)S(1)}, f32[2,128,256]{2,1,0:T(8,128)}, u32[]{:S(2)}) copy-start(f32[2,128,256]{2,1,0:T(8,128)} %custom-call.2) | copy-start | bytes 786436
  179.8 15.6 %copy-start.6 = (f32[2,128,256]{2,1,0:T(8,128)S(1)}, f32[2,128,256]{2,1,0:T(8,128)}, u32[]{:S(2)}) copy-start(f32[2,128,256]{2,1,0:T(8,128)} %copy-done.5) | copy-start | bytes 786436
  179.8 17.7 %copy-start.19 = (f32[512]{0:T(512)S(1)}, f32[512]{0:T(512)}, u32[]{:S(2)}) copy-start(f32[512]{0:T(512)} %param.44) | copy-start | bytes 6148
  187.0 8.4 %copy-start.12 = (f32[128,2,256]{0,2,1:T(8,128)S(1)}, f32[128,2,256]{0,2,1:T(8,128)}, u32[]{:S(2)}) copy-start(f32[128,2,256]{0,2,1:T(8,128)} %rev.38) | copy-start | bytes 786436
  187.0 12.2 %copy-start.20 = (f32[2,512]{1,0:T(2,128)S(1)}, f32[2,512]{1,0:T(2,128)}, u32[]{:S(2)}) copy-start(f32[2,512]{1,0:T(2,128)} %get-tuple-element.705) | copy-start | bytes 12292
  187.0 49.0 %copy-start.11 = (bf16[128,512]{1,0:T(8,128)(2,1)S(1)}, bf16[128,512]{1,0:T(8,128)(2,1)}, u32[]{:S(2)}) copy-start(bf16[128,512]{1,0:T(8,128)(2,1)} %param.29) | copy-start | bytes 393220
Sparse Core Ops, SparseCore 0:
  51.5 36.7 all-gather.6
  199.3 36.6 all-gather.8
